TPU v7x, 512 devices: a whole 4x4x16 slice. The times are simulated.
512 devices in a mesh: sp: 64 (over z, y), tp: 8 (over x, core).
Axes of the slice: x: 4, y: 4, z: 16, core: 2. Of those that a mesh axis runs over, the one named last changes fastest.
Arguments:
- resid: bfloat16 [16384, 2048], P(('sp', 'tp')), may hold values from -6 to 6
- queries: bfloat16 [16384, 1024], P('sp', 'tp'), may hold values from -6 to 6
- keys: bfloat16 [512, 16384], P('tp', 'sp'), may hold values from -6 to 6
- values: bfloat16 [512, 16384], P('tp', 'sp'), may hold values from -6 to 6
- log_gates: float32 [16, 16384], P('tp', 'sp'), may hold values from -1640 to 0, as said below
- q_gain: float32 [64], replicated, may hold values from 0.5 to 7
- k_gain: float32 [64], replicated, may hold values from 0.5 to 7
- w_out: bfloat16 [1024, 2048], P('tp'), may hold values from -0.1875 to 0.1875
- mlp_gain: bfloat16 [2048], replicated, may hold values from 0.099609375 to 1.8984375
- w_up: bfloat16 [2048, 8192], P('sp', 'tp'), may hold values from -0.125 to 0.125
- w_down: bfloat16 [8192, 2048], P('tp', 'sp'), may hold values from -0.0625 to 0.0625
Outputs:
- output: bfloat16 [16384, 2048], P(('sp', 'tp'))
Inputs may be any that keep to these rules, and one draw needn't show every extreme that they name: `log_gates`: each head's values never rise along positions.
All inputs are finite; a program needn't handle non-finite values.
Results may differ from a plain program's by a relative error of at most 0.018.
The roundings to bfloat16 on the way count: a program that leaves them out, or rounds other values in their place, can miss the bound.
Values may be sent and summed in bfloat16 or wider, within the bound.
No kernel may reach another device: no remote copies, remote signals or barrier semaphores. Data moves between devices by JAX's collectives and lax.ppermute only.
A program may use at most 64 MiB of HBM per device.

v0:
```python
import math
import jax
import jax.numpy as jnp
from jax import lax
from jax.sharding import PartitionSpec as P

EPS = 1e-06


def rows_first(arrays, axis, dims):
    turned = [jnp.moveaxis(a, dim, 0) for a, dim in zip(arrays, dims)]
    widths = [t[0].size for t in turned]
    both = jnp.concatenate([t.reshape(-1, w) for t, w in zip(turned, widths)], axis=1)
    result = lax.all_gather(both, axis, axis=0, tiled=True)
    parts = jnp.split(result, [sum(widths[:k]) for k in range(1, len(widths))], axis=1)
    return tuple(
        (
            jnp.moveaxis(b.reshape(-1, *t.shape[1:]), 0, dim)
            for b, t, dim in zip(parts, turned, dims)
        )
    )


def sent_to_all(value, axis):
    count = lax.axis_size(axis)
    return lax.all_to_all(
        jnp.broadcast_to(value[None], (count, *value.shape)), axis, 0, 0, tiled=True
    )


def joined_along(parts, dim):
    lengths = list(parts.shape[1:])
    lengths[dim] *= parts.shape[0]
    return jnp.moveaxis(parts, 0, dim).reshape(lengths)


def gather_directly(value, axis, dim):
    parts = sent_to_all(value, axis)
    return joined_along(parts, dim)


def in_one_piece(arrays, axis, dim, along):
    ends, at = ([], 0)
    for a in arrays[:-1]:
        at += a.shape[along]
        ends.append(at)
    both = jnp.concatenate(arrays, axis=along)
    return tuple(jnp.split(lax.all_gather(both, axis, axis=dim, tiled=True), ends, axis=along))


def cut_along(value, dim, count):
    before, after = (value.shape[:dim], value.shape[dim + 1 :])
    return jnp.moveaxis(value.reshape(*before, count, -1, *after), dim, 0)


def summed_on_arrival(value, axis, dim):
    count = lax.axis_size(axis)
    parts = lax.all_to_all(cut_along(value, dim, count), axis, 0, 0, tiled=True)
    return jnp.sum(parts.astype(jnp.float32), axis=0)


def rms_last(input_values, gain):
    scale = lax.rsqrt(jnp.mean(input_values * input_values, axis=-1, keepdims=True) + EPS)
    return input_values * scale * gain


def local(resid, queries, keys, values, log_gates, q_gain, k_gain, w_out, mlp_gain, w_up, w_down):
    up_whole, down_whole = rows_first((w_up, w_down), "sp", (0, 1))
    positions = queries.shape[0]
    head_size = q_gain.shape[0]
    query_count = log_gates.shape[0]
    key_total_count = keys.shape[0] // head_size
    group = query_count // key_total_count
    query_heads = queries.astype(jnp.float32).reshape(positions, query_count, head_size)
    qnorm = (rms_last(query_heads, q_gain) * head_size ** (-0.5)).astype(jnp.bfloat16)
    qnorm = jnp.transpose(qnorm.reshape(positions, key_total_count, group, head_size), (1, 2, 0, 3))
    key_heads = keys.astype(jnp.float32).reshape(key_total_count, head_size, positions)
    key_scale = lax.rsqrt(jnp.mean(key_heads * key_heads, axis=1, keepdims=True) + EPS)
    knorm = (key_heads * key_scale * k_gain[None, :, None]).astype(jnp.bfloat16)
    knorm = knorm.reshape(key_total_count * head_size, positions)
    gates_all = gather_directly(log_gates, "sp", 1)
    offset = lax.axis_index("sp") * positions
    query_pos = offset + jnp.arange(positions, dtype=jnp.int32)
    query_last = offset + positions - 1
    query_gates = log_gates.reshape(key_total_count, group, positions)
    start_state = (
        jnp.full((key_total_count, group, positions), -1e30, jnp.float32),
        jnp.zeros((key_total_count, group, positions), jnp.float32),
        jnp.zeros((key_total_count, group, positions, head_size), jnp.float32),
    )
    key_piece, value_piece = in_one_piece((knorm, values), "sp", 1, 0)
    length = key_piece.shape[1]
    block = math.gcd(length, 1024)
    key_blocks = key_piece.reshape(key_total_count, head_size, length)
    value_blocks = value_piece.reshape(key_total_count, head_size, length)

    def one_step(index, state):
        first = index * block

        def compute(inner):
            running_top, running_total, running_sum = inner
            key_now = lax.dynamic_slice_in_dim(key_blocks, index * block, block, 2)
            value_now = lax.dynamic_slice_in_dim(value_blocks, index * block, block, 2)
            gates_now = lax.dynamic_slice_in_dim(gates_all, first, block, 1).reshape(
                key_total_count, group, block
            )
            logits = jnp.einsum(
                "kgtd,kdn->kgtn", qnorm, key_now, preferred_element_type=jnp.float32
            )
            logits = logits + query_gates[..., None] - gates_now[:, :, None, :]
            key_pos = first + jnp.arange(block, dtype=jnp.int32)
            logits = jnp.where(key_pos[None, :] <= query_pos[:, None], logits, -jnp.inf)
            new_top = jnp.maximum(running_top, jnp.max(logits, axis=-1))
            rescale = jnp.exp(running_top - new_top)
            weights = jnp.exp(logits - new_top[..., None])
            new_total = running_total * rescale + jnp.sum(weights, axis=-1)
            product = jnp.einsum(
                "kgtn,kdn->kgtd",
                weights.astype(jnp.bfloat16),
                value_now,
                preferred_element_type=jnp.float32,
            )
            return (new_top, new_total, running_sum * rescale[..., None] + product)

        return lax.cond(first <= query_last, compute, lambda inner: inner, state)

    final_top, final_total, final_sum = lax.fori_loop(0, length // block, one_step, start_state)
    attn = final_sum / final_total[..., None]
    attn = (
        jnp.transpose(attn, (2, 0, 1, 3))
        .reshape(positions, query_count * head_size)
        .astype(jnp.bfloat16)
    )
    rows_now = attn
    proj = summed_on_arrival(
        jnp.dot(rows_now, w_out, preferred_element_type=jnp.float32).astype(jnp.bfloat16), "tp", 0
    )
    mixed = (resid.astype(jnp.float32) + proj).astype(jnp.bfloat16)
    normed = rms_last(mixed.astype(jnp.float32), mlp_gain.astype(jnp.float32)).astype(jnp.bfloat16)
    upward = jnp.dot(gather_directly(normed, "tp", 0), up_whole, preferred_element_type=jnp.float32)
    act = jnp.square(jax.nn.relu(upward)).astype(jnp.bfloat16)
    rows_now = act
    summed_down = summed_on_arrival(
        jnp.dot(rows_now, down_whole, preferred_element_type=jnp.float32).astype(jnp.bfloat16),
        "tp",
        0,
    )
    return (mixed.astype(jnp.float32) + summed_down).astype(jnp.bfloat16)


def solution(mesh):
    return jax.shard_map(
        local,
        mesh=mesh,
        in_specs=(
            P(("sp", "tp"), None),
            P("sp", "tp"),
            P("tp", "sp"),
            P("tp", "sp"),
            P("tp", "sp"),
            P(),
            P(),
            P("tp", None),
            P(),
            P("sp", "tp"),
            P("tp", "sp"),
        ),
        out_specs=P(("sp", "tp"), None),
        check_vma=False,
    )
```

profile of v0, /device:TPU:1, one launch (start us, length us, event | category | flops | bytes accessed | tf_op | source)
XLA Modules:
  0.0 348.9 jit_solution(38273085295830202)
XLA Ops:
  6.5 0.0 copy-start
  6.5 0.0 all-gather.3.cloned.1.call-start
  6.5 0.8 fusion.39
  7.4 0.8 fusion.41
  8.2 1.4 pad_maximum_fusion.1
  9.6 0.0 all-gather.3.cloned.1.call-update
  9.6 0.0 all-gather.5.cloned.1.call-start
  9.7 1.5 pad_maximum_fusion
  11.2 0.0 all-gather.5.cloned.1.call-update
  11.3 1.4 broadcast_in_dim.25
  12.6 19.3 %all-to-all-start = ((f32[64,2,256]{2,1,0:T(2,128)}), f32[64,2,256]{2,1,0:T(2,128)S(1)}, u32[]{:S(2)}, u32[]{:S(2)}) async-start(f32[64,2,256]{2,1,0:T(2,128)} %broadcast_in_dim.25), calls=%async_computation | async-start | bytes 262144 | tf_op jit(solution)/shard_map/all_to_all | solution.py:26
  31.9 0.9 copy.17
  32.9 0.7 fusion.42
  33.6 0.0 copy-start.3
  33.7 119.0 %all-gather.3.cloned.1.call-done = bf16[128,16384]{1,0:T(8,128)(2,1)} async-done(((bf16[128,256]{1,0:T(8,128)(2,1)}), bf16[128,16384]{1,0:T(8,128)(2,1)}) %all-gather.3.cloned.1.call-update) | async-done | bytes 4194320 | tf_op jit(solution)/shard_map/all_gather | solution.py:48
  152.6 3.9 %slice_bitcast_fusion = (bf16[1,64,16384]{2,1,0:T(8,128)(2,1)S(1)}, bf16[1,64,16384]{2,1,0:T(8,128)(2,1)}) fusion(bf16[128,16384]{1,0:T(8,128)(2,1)} %all-gather.3.cloned.1.call-done), kind=kLoop, calls=%fused_computation.30 | loop fusion | bytes 8388608 | tf_op jit(solution)/shard_map/reshape | solution.py:95
  156.5 0.0 all-to-all-done
  156.6 0.0 copy-done.3
  156.6 3.4 while.18
  156.6 2.6 conditional.3
  156.7 0.2 broadcast_compare_fusion
  156.9 1.5 fusion.44
  158.4 0.5 fusion.5
  158.9 0.3 fusion.4
  160.0 0.0 copy-start.2
  160.1 0.0 copy-done
  160.1 1.5 convolution_convert_fusion
  161.6 0.0 copy-start.1
  161.6 14.5 %all-to-all-start.1 = ((bf16[8,32,2048]{2,1,0:T(8,128)(2,1)}), bf16[8,32,2048]{2,1,0:T(8,128)(2,1)S(1)}, u32[]{:S(2)}, u32[]{:S(2)}) async-start(bf16[8,32,2048]{2,1,0:T(8,128)(2,1)} %bitcast.21), calls=%async_computation.1 | async-start | bytes 2097152 | tf_op jit(solution)/shard_map/all_to_all | solution.py:58
  176.1 0.0 copy-done.2
  176.1 15.0 %all-to-all-done.1 = bf16[8,32,2048]{2,1,0:T(8,128)(2,1)S(1)} async-done(((bf16[8,32,2048]{2,1,0:T(8,128)(2,1)}), bf16[8,32,2048]{2,1,0:T(8,128)(2,1)S(1)}, u32[]{:S(2)}, u32[]{:S(2)}) %all-to-all-start.1) | async-done | bytes 1048608 | tf_op jit(solution)/shard_map/all_to_all | solution.py:58
  191.1 0.1 convert_reduce_fusion.1
  191.2 0.0 copy-done.1
  191.2 0.2 fusion.35
  191.4 0.1 fusion.37
  191.5 0.1 broadcast_in_dim.26
  191.6 18.3 %all_to_all.20 = bf16[8,32,2048]{2,1,0:T(8,128)(2,1)S(1)} all-to-all(bf16[8,32,2048]{2,1,0:T(8,128)(2,1)S(1)} %broadcast_in_dim.26), channel_id=1, replica_groups=mesh['sp'=64,'tp'=8] {'tp'}, dimensions={0} | all-to-all | bytes 2097152 | tf_op jit(solution)/shard_map/all_to_all | solution.py:26
  209.9 98.1 %all-gather.5.cloned.1.call-done = bf16[2048,2048]{1,0:T(8,128)(2,1)} async-done(((bf16[32,2048]{1,0:T(8,128)(2,1)}), bf16[2048,2048]{1,0:T(8,128)(2,1)}) %all-gather.5.cloned.1.call-update) | async-done | bytes 8388624 | tf_op jit(solution)/shard_map/all_gather | solution.py:14
  308.0 5.8 %fusion.20 = bf16[256,2048]{1,0:T(8,128)(2,1)S(1)} fusion(bf16[2048,2048]{1,0:T(8,128)(2,1)} %all-gather.5.cloned.1.call-done, bf16[256,2048]{1,0:T(8,128)(2,1)S(1)} %bitcast.57), kind=kOutput, calls=%fused_computation.29 | convolution fusion | flops 2148794368 | bytes 10485760 | tf_op jit(solution)/shard_map/dot_general | solution.py:144
  313.9 27.4 %all_to_all.21 = bf16[8,32,2048]{2,1,0:T(8,128)(2,1)S(1)} all-to-all(bf16[8,32,2048]{2,1,0:T(8,128)(2,1)S(1)} %bitcast.58), channel_id=1, replica_groups=mesh['sp'=64,'tp'=8] {'tp'}, dimensions={0} | all-to-all | bytes 2097152 | tf_op jit(solution)/shard_map/all_to_all | solution.py:58
  341.3 0.1 convert_reduce_fusion
  341.4 0.7 fusion.38
  (46 shorter events, 0.3 us)
Async XLA Ops:
  6.5 153.5 %copy-start = (bf16[128,2048]{1,0:T(8,128)(2,1)S(1)}, bf16[128,2048]{1,0:T(8,128)(2,1)}, u32[]{:S(2)}) copy-start(bf16[128,2048]{1,0:T(8,128)(2,1)} %param.22) | copy-start | bytes 1572868
  6.5 146.1 %all-gather.3.cloned.1.call-start = ((), (), s32[]{:S(2)}) async-start(), calls=%async_computation.4 | async-start | bytes 4259840 | tf_op jit(solution)/shard_map/all_gather | solution.py:48
  9.6 298.4 %all-gather.5.cloned.1.call-start = ((), (), s32[]{:S(2)}) async-start(), calls=%async_computation.5 | async-start | bytes 8519680 | tf_op jit(solution)/shard_map/all_gather | solution.py:14
  12.6 143.9 %all-to-all-start = ((f32[64,2,256]{2,1,0:T(2,128)}), f32[64,2,256]{2,1,0:T(2,128)S(1)}, u32[]{:S(2)}, u32[]{:S(2)}) async-start(f32[64,2,256]{2,1,0:T(2,128)} %broadcast_in_dim.25), calls=%async_computation | async-start | bytes 262144 | tf_op jit(solution)/shard_map/all_to_all | solution.py:26
  33.6 122.9 %copy-start.3 = (f32[2,256]{1,0:T(2,128)S(1)}, f32[2,256]{1,0:T(2,128)}, u32[]{:S(2)}) copy-start(f32[2,256]{1,0:T(2,128)} %param.19) | copy-start | bytes 6148
  160.0 16.1 %copy-start.2 = (bf16[2048]{0:T(1024)(128)(2,1)S(1)}, bf16[2048]{0:T(1024)(128)(2,1)}, u32[]{:S(2)}) copy-start(bf16[2048]{0:T(1024)(128)(2,1)} %param.23) | copy-start | bytes 12292
  161.6 29.6 %copy-start.1 = (bf16[32,2048]{1,0:T(8,128)(2,1)S(1)}, bf16[32,2048]{1,0:T(8,128)(2,1)}, u32[]{:S(2)}) copy-start(bf16[32,2048]{1,0:T(8,128)(2,1)} %param.15) | copy-start | bytes 393220
  161.6 29.5 %all-to-all-start.1 = ((bf16[8,32,2048]{2,1,0:T(8,128)(2,1)}), bf16[8,32,2048]{2,1,0:T(8,128)(2,1)S(1)}, u32[]{:S(2)}, u32[]{:S(2)}) async-start(bf16[8,32,2048]{2,1,0:T(8,128)(2,1)} %bitcast.21), calls=%async_computation.1 | async-start | bytes 2097152 | tf_op jit(solution)/shard_map/all_to_all | solution.py:58
Sparse Core Ops, SparseCore 0:
  10.2 142.3 all-gather.2
  155.6 152.4 all-gather.4
where the time goes:
time: 350 us; the launch traced here: 349 us
  waiting for transfers between devices  232 us (66%)
  blocking collectives  45.7 us (13%)
  starting transfers between devices  33.8 us (10%)
  between operations  13.6 us (4%)
  matrix products  9.29 us (3%)
  other arithmetic  7.18 us (2%)
  local copies, waits for them, and re-layouts  6.37 us (2%)
    all_gather x1, waiting for transfers between devices, in_one_piece(): lax.all_gather(both, axis, axis=dim, tiled=True)  119 us
    all_gather x1, waiting for transfers between devices, rows_first(): result = lax.all_gather(both, axis, axis=0, tiled=True)  98.1 us
    all_to_all x1, blocking collectives, summed_on_arrival(): parts = lax.all_to_all(cut_along(value, dim, count), axis, 0, 0, tiled=True)  27.4 us
    all_to_all x1, starting transfers between devices, sent_to_all(): lax.all_to_all(jnp.broadcast_to(value[None], (count, *value.shape)), axis...  19.3 us
    all_to_all x1, blocking collectives, sent_to_all(): lax.all_to_all(jnp.broadcast_to(value[None], (count, *value.shape)), axis...  18.3 us
    all_to_all x1, waiting for transfers between devices, summed_on_arrival(): parts = lax.all_to_all(cut_along(value, dim, count), axis, 0, 0, tiled=True)  15 us
    all_to_all x1, starting transfers between devices, summed_on_arrival(): parts = lax.all_to_all(cut_along(value, dim, count), axis, 0, 0, tiled=True)  14.5 us
  transfers between devices with their start and end apart: 4, of which 3 were waited for; matrix products, arithmetic and copies ran while one was open for 4% of the time, Pallas kernels for 0%

commit v1 on v0

--- a/solution.py
+++ b/solution.py
@@ -11,7 +11,9 @@
     turned = [jnp.moveaxis(a, dim, 0) for a, dim in zip(arrays, dims)]
     widths = [t[0].size for t in turned]
     both = jnp.concatenate([t.reshape(-1, w) for t, w in zip(turned, widths)], axis=1)
-    result = lax.all_gather(both, axis, axis=0, tiled=True)
+    result = jnp.concatenate(
+        lax.all_to_all(jnp.stack([both] * lax.axis_size(axis)), axis, 0, 0), axis=0
+    )
     parts = jnp.split(result, [sum(widths[:k]) for k in range(1, len(widths))], axis=1)
     return tuple(
         (

time: 350 us -> 660 us (1.89)
  blocking collectives: 45.7 us -> 432 us
  waiting for transfers between devices: 232 us -> 150 us
    all_to_all x1, blocking collectives: 18.3 us -> 409 us  [rows_first(): lax.all_to_all(jnp.stack([both] * lax.axis_size(axis)), axis, 0, 0)]
    all_gather x1 -> x0, waiting for transfers between devices: 98.1 us -> none  [rows_first(): result = lax.all_gather(both, axis, axis=0, tiled=True)]
    all_to_all x1 -> x2, waiting for transfers between devices: 0.01 us -> 15 us  [sent_to_all(): lax.all_to_all(jnp.broadcast_to(value[None], (count, *value.shape)), axis...]
    all_to_all x1 -> x2, starting transfers between devices: 19.3 us -> 23.7 us  [sent_to_all(): lax.all_to_all(jnp.broadcast_to(value[None], (count, *value.shape)), axis...]
  transfers between devices with their start and end apart: 4 -> 4, of which waited for: 3 -> 3; matrix products, arithmetic and copies ran while one was open for 4% -> 1% of each run, Pallas kernels for 0% -> 0%
where the time goes in v1:
time: 660 us; the launch traced here: 659 us
  blocking collectives  432 us (65%)
  waiting for transfers between devices  150 us (23%)
  starting transfers between devices  38.2 us (6%)
  between operations  13.6 us (2%)
  matrix products  9.21 us (1%)
  local copies, waits for them, and re-layouts  8.41 us (1%)
    all_to_all x1, blocking collectives, rows_first(): lax.all_to_all(jnp.stack([both] * lax.axis_size(axis)), axis, 0, 0)  409 us
    all_gather x1, waiting for transfers between devices, in_one_piece(): lax.all_gather(both, axis, axis=dim, tiled=True)  120 us
    all_to_all x1, blocking collectives, summed_on_arrival(): parts = lax.all_to_all(cut_along(value, dim, count), axis, 0, 0, tiled=True)  23.8 us
    all_to_all x2, starting transfers between devices, sent_to_all(): lax.all_to_all(jnp.broadcast_to(value[None], (count, *value.shape)), axis...  23.7 us
    all_to_all x2, waiting for transfers between devices, sent_to_all(): lax.all_to_all(jnp.broadcast_to(value[None], (count, *value.shape)), axis...  15 us
    all_to_all x1, waiting for transfers between devices, summed_on_arrival(): parts = lax.all_to_all(cut_along(value, dim, count), axis, 0, 0, tiled=True)  15 us
    all_to_all x1, starting transfers between devices, summed_on_arrival(): parts = lax.all_to_all(cut_along(value, dim, count), axis, 0, 0, tiled=True)  14.5 us
  transfers between devices with their start and end apart: 4, of which 3 were waited for; matrix products, arithmetic and copies ran while one was open for 1% of the time, Pallas kernels for 0%

profile of v1, /device:TPU:1, one launch (start us, length us, event | category | flops | bytes accessed | tf_op | source)
XLA Modules:
  0.0 658.8 jit_solution(7782676902349739408)
XLA Ops:
  6.5 0.0 copy-start
  6.5 0.0 all-gather.2.cloned.1.call-start
  6.5 0.8 fusion.39
  7.4 0.8 fusion.41
  8.2 1.4 pad_maximum_fusion.1
  9.6 0.0 all-gather.2.cloned.1.call-update
  9.6 1.4 broadcast_in_dim.25
  11.0 19.3 %all-to-all-start = ((f32[64,2,256]{2,1,0:T(2,128)}), f32[64,2,256]{2,1,0:T(2,128)S(1)}, u32[]{:S(2)}, u32[]{:S(2)}) async-start(f32[64,2,256]{2,1,0:T(2,128)} %broadcast_in_dim.25), calls=%async_computation | async-start | bytes 262144 | tf_op jit(solution)/shard_map/all_to_all | solution.py:28
  30.3 0.9 copy.17
  31.3 0.7 fusion.42
  32.0 0.0 copy-start.5
  32.1 120.4 %all-gather.2.cloned.1.call-done = bf16[128,16384]{1,0:T(8,128)(2,1)} async-done(((bf16[128,256]{1,0:T(8,128)(2,1)}), bf16[128,16384]{1,0:T(8,128)(2,1)}) %all-gather.2.cloned.1.call-update) | async-done | bytes 4194320 | tf_op jit(solution)/shard_map/all_gather | solution.py:50
  152.5 3.9 slice_bitcast_fusion
  156.3 0.0 all-to-all-done
  156.4 0.0 copy-done.5
  156.4 3.5 while.18
  156.4 2.6 conditional.3
  156.5 0.2 broadcast_compare_fusion
  156.7 1.5 fusion.44
  158.2 0.3 fusion.4
  158.5 0.5 fusion.5
  159.9 0.0 copy-start.4
  159.9 0.0 copy-done
  159.9 1.4 convolution_convert_fusion
  161.3 0.0 copy-start.1
  161.3 14.5 %all-to-all-start.1 = ((bf16[8,32,2048]{2,1,0:T(8,128)(2,1)}), bf16[8,32,2048]{2,1,0:T(8,128)(2,1)S(1)}, u32[]{:S(2)}, u32[]{:S(2)}) async-start(bf16[8,32,2048]{2,1,0:T(8,128)(2,1)} %bitcast.21), calls=%async_computation.1 | async-start | bytes 2097152 | tf_op jit(solution)/shard_map/all_to_all | solution.py:60
  175.9 0.0 copy-done.4
  175.9 15.0 %all-to-all-done.1 = bf16[8,32,2048]{2,1,0:T(8,128)(2,1)S(1)} async-done(((bf16[8,32,2048]{2,1,0:T(8,128)(2,1)}), bf16[8,32,2048]{2,1,0:T(8,128)(2,1)S(1)}, u32[]{:S(2)}, u32[]{:S(2)}) %all-to-all-start.1) | async-done | bytes 1048608 | tf_op jit(solution)/shard_map/all_to_all | solution.py:60
  190.9 0.1 convert_reduce_fusion.1
  191.0 0.0 copy-done.1
  191.0 0.0 copy-start.2
  191.0 0.0 copy-start.3
  191.0 0.2 fusion.35
  191.2 0.1 fusion.37
  191.3 1.1 broadcast_in_dim.26
  192.4 4.4 all-to-all-start.2
  196.8 0.0 copy-done.2
  196.8 0.0 copy-done.3
  196.9 15.0 %all-to-all-done.2 = bf16[8,32,2048]{2,1,0:T(8,128)(2,1)S(1)} async-done(((bf16[8,32,2048]{2,1,0:T(8,128)(2,1)}), bf16[8,32,2048]{2,1,0:T(8,128)(2,1)S(1)}, u32[]{:S(2)}, u32[]{:S(2)}) %all-to-all-start.2) | async-done | bytes 1048608 | tf_op jit(solution)/shard_map/all_to_all | solution.py:28
  211.8 1.1 stack.2
  212.9 408.6 %all_to_all.25 = bf16[64,32,2048]{2,1,0:T(8,128)(2,1)} all-to-all(bf16[64,32,2048]{2,1,0:T(8,128)(2,1)S(1)} %stack.2), channel_id=1, replica_groups=mesh['sp'=64,'tp'=8] {'sp'}, dimensions={0} | all-to-all | bytes 16777216 | tf_op jit(solution)/shard_map/all_to_all | solution.py:15
  621.5 5.8 fusion.20
  627.3 23.8 %all_to_all.26 = bf16[8,32,2048]{2,1,0:T(8,128)(2,1)S(1)} all-to-all(bf16[8,32,2048]{2,1,0:T(8,128)(2,1)S(1)} %bitcast.60), channel_id=1, replica_groups=mesh['sp'=64,'tp'=8] {'tp'}, dimensions={0} | all-to-all | bytes 2097152 | tf_op jit(solution)/shard_map/all_to_all | solution.py:60
  651.1 0.1 convert_reduce_fusion
  651.3 0.7 fusion.38
  (47 shorter events, 0.4 us)
Async XLA Ops:
  6.5 153.4 %copy-start = (bf16[128,2048]{1,0:T(8,128)(2,1)S(1)}, bf16[128,2048]{1,0:T(8,128)(2,1)}, u32[]{:S(2)}) copy-start(bf16[128,2048]{1,0:T(8,128)(2,1)} %param.22) | copy-start | bytes 1572868
  6.5 145.9 %all-gather.2.cloned.1.call-start = ((), (), s32[]{:S(2)}) async-start(), calls=%async_computation.5 | async-start | bytes 4259840 | tf_op jit(solution)/shard_map/all_gather | solution.py:50
  11.0 145.3 %all-to-all-start = ((f32[64,2,256]{2,1,0:T(2,128)}), f32[64,2,256]{2,1,0:T(2,128)S(1)}, u32[]{:S(2)}, u32[]{:S(2)}) async-start(f32[64,2,256]{2,1,0:T(2,128)} %broadcast_in_dim.25), calls=%async_computation | async-start | bytes 262144 | tf_op jit(solution)/shard_map/all_to_all | solution.py:28
  32.0 124.3 %copy-start.5 = (f32[2,256]{1,0:T(2,128)S(1)}, f32[2,256]{1,0:T(2,128)}, u32[]{:S(2)}) copy-start(f32[2,256]{1,0:T(2,128)} %param.19) | copy-start | bytes 6148
  159.9 16.0 %copy-start.4 = (bf16[2048]{0:T(1024)(128)(2,1)S(1)}, bf16[2048]{0:T(1024)(128)(2,1)}, u32[]{:S(2)}) copy-start(bf16[2048]{0:T(1024)(128)(2,1)} %param.23) | copy-start | bytes 12292
  161.3 29.7 %copy-start.1 = (bf16[32,2048]{1,0:T(8,128)(2,1)S(1)}, bf16[32,2048]{1,0:T(8,128)(2,1)}, u32[]{:S(2)}) copy-start(bf16[32,2048]{1,0:T(8,128)(2,1)} %param.15) | copy-start | bytes 393220
  161.3 29.5 %all-to-all-start.1 = ((bf16[8,32,2048]{2,1,0:T(8,128)(2,1)}), bf16[8,32,2048]{2,1,0:T(8,128)(2,1)S(1)}, u32[]{:S(2)}, u32[]{:S(2)}) async-start(bf16[8,32,2048]{2,1,0:T(8,128)(2,1)} %bitcast.21), calls=%async_computation.1 | async-start | bytes 2097152 | tf_op jit(solution)/shard_map/all_to_all | solution.py:60
  191.0 5.8 copy-start.2
  191.0 5.8 copy-start.3
  192.4 19.4 %all-to-all-start.2 = ((bf16[8,32,2048]{2,1,0:T(8,128)(2,1)}), bf16[8,32,2048]{2,1,0:T(8,128)(2,1)S(1)}, u32[]{:S(2)}, u32[]{:S(2)}) async-start(bf16[8,32,2048]{2,1,0:T(8,128)(2,1)} %broadcast_in_dim.26), calls=%async_computation.2 | async-start | bytes 2097152 | tf_op jit(solution)/shard_map/all_to_all | solution.py:28
Sparse Core Ops, SparseCore 0:
  10.2 142.1 all-gather.1
